TPU v7x, 32 devices: a whole 2x2x4 slice. The times are simulated.
32 devices in a mesh: ep: 8 (over z, core), tp: 4 (over y, x).
Axes of the slice: x: 2, y: 2, z: 4, core: 2. Of those that a mesh axis runs over, the one named last changes fastest.
Arguments:
- tokens: bfloat16 [1024, 3072], P('ep', 'tp'), may hold values from -6 to 6
- routes: int32 [1024, 2], P('ep'), may hold values from 0 to 7, all different within a row; in each aligned block of 128 rows (0 to 127, 128 to 255, ...) at most 40 rows name the same one
- gates: float32 [1024, 2], P('ep'), may hold values from 0.1 to 1.5
- cotangent: bfloat16 [1024, 3072], P('ep', 'tp'), may hold values from -6 to 6
- w_gate: bfloat16 [8, 3072, 896], P('ep', 'tp'), may hold values from -0.109375 to 0.109375
- w_up: bfloat16 [8, 3072, 896], P('ep', 'tp'), may hold values from -0.109375 to 0.109375
- w_down: bfloat16 [8, 3072, 896], P('ep', 'tp'), may hold values from -0.1875 to 0.1875
- shared_hidden: bfloat16 [1024, 448], P('ep'), may hold values from -0.2362278 to 0.2362278
Outputs:
- token_grad: bfloat16 [1024, 3072], P('ep', 'tp')
- gate_grad: float32 [1024, 2], P('ep')
- grad_w_gate: float32 [8, 3072, 896], P('ep', 'tp')
- grad_w_up: float32 [8, 3072, 896], P('ep', 'tp')
- grad_w_down: float32 [8, 3072, 896], P('ep', 'tp')
- row_norms: float32 [3, 8, 3072], P(None, 'ep', 'tp')
- grad_shared: float32 [3072, 448], P('tp', 'ep')
- shared_norms: float32 [3072], P('tp')
Inputs may be any that keep to these rules, and one draw needn't show every extreme that they name: `routes`: in each aligned block of 128 rows (the tokens of one index of ep) a row names 2 different experts and no expert is named by more than 40 rows; some expert is named by exactly 40 rows in some blocks.
All inputs are finite; a program needn't handle non-finite values.
Results may differ from a plain program's by a relative error of at most 0.024.
Values may be sent and summed in bfloat16 or wider, within the bound.
A program may use at most 64 MiB of HBM per device.

v0:
```python
import jax
import jax.numpy as jnp
from jax import lax
from jax.sharding import PartitionSpec as P


def slot_targets(routes, experts, capacity):
    chosen = routes.reshape(-1)
    onehot = (chosen[:, None] == jnp.arange(experts, dtype=jnp.int32)[None, :]).astype(jnp.int32)
    earlier = jnp.cumsum(onehot, axis=0) - onehot
    position = jnp.sum(earlier * onehot, axis=1)
    return chosen * capacity + position


def expert_math(gate_sum, up_sum, down_sum):
    sigma = jax.nn.sigmoid(gate_sum)
    active = gate_sum * sigma
    hidden = (active * up_sum).astype(jnp.bfloat16)
    product = jnp.sum(active * up_sum * down_sum, axis=-1).astype(jnp.bfloat16)
    gate_back = (down_sum * up_sum * sigma * (1.0 + gate_sum * (1.0 - sigma))).astype(jnp.bfloat16)
    up_back = (down_sum * active).astype(jnp.bfloat16)
    return (hidden, gate_back, up_back, product)


def on_device(tokens, routes, gates, cotangent, w_gate, w_up, w_down, shared_hidden):
    tok_count, width_part = tokens.shape
    top_count = routes.shape[1]
    local_experts = w_gate.shape[0]
    experts = local_experts * lax.axis_size("ep")
    capacity = 5 * tok_count * top_count // (4 * experts)
    pair_count = tok_count * top_count
    target = slot_targets(routes, experts, capacity)
    source = (
        jnp.zeros((experts * capacity,), jnp.int32)
        .at[target]
        .set(jnp.arange(pair_count, dtype=jnp.int32))
    )
    filled = jnp.zeros((experts * capacity,), jnp.bool_).at[target].set(True)
    scaled = (gates[:, :, None] * cotangent[:, None, :].astype(jnp.float32)).astype(jnp.bfloat16)
    scaled = scaled.reshape(pair_count, width_part)
    zero_row = jnp.zeros((), jnp.bfloat16)
    token_rows = jnp.where(filled[:, None], tokens[source // top_count], zero_row)
    grad_rows = jnp.where(filled[:, None], scaled[source], zero_row)
    token_rows = token_rows.reshape(experts, capacity, width_part)
    grad_rows = grad_rows.reshape(experts, capacity, width_part)
    arrived_tok, arrived_grad = (
        lax.all_to_all(token_rows, "ep", split_axis=0, concat_axis=1, tiled=True),
        lax.all_to_all(grad_rows, "ep", split_axis=0, concat_axis=1, tiled=True),
    )
    gate_part = jnp.einsum("erd,edf->erf", arrived_tok, w_gate, preferred_element_type=jnp.float32)
    up_part = jnp.einsum("erd,edf->erf", arrived_tok, w_up, preferred_element_type=jnp.float32)
    down_part = jnp.einsum("erd,edf->erf", arrived_grad, w_down, preferred_element_type=jnp.float32)
    sums = (
        lax.psum(gate_part.astype(jnp.bfloat16), "tp").astype(jnp.float32),
        lax.psum(up_part.astype(jnp.bfloat16), "tp").astype(jnp.float32),
        lax.psum(down_part.astype(jnp.bfloat16), "tp").astype(jnp.float32),
    )
    hidden, gate_back, up_back, product = expert_math(sums[0], sums[1], sums[2])
    grad_gate = jnp.einsum(
        "erd,erf->edf", arrived_tok, gate_back, preferred_element_type=jnp.float32
    )
    grad_up = jnp.einsum("erd,erf->edf", arrived_tok, up_back, preferred_element_type=jnp.float32)
    grad_down = jnp.einsum("erd,erf->edf", arrived_grad, hidden, preferred_element_type=jnp.float32)
    token_back = jnp.einsum(
        "erf,edf->erd", gate_back, w_gate, preferred_element_type=jnp.float32
    ) + jnp.einsum("erf,edf->erd", up_back, w_up, preferred_element_type=jnp.float32)
    token_back = token_back.astype(jnp.bfloat16)
    back_rows, back_product = (
        lax.all_to_all(token_back, "ep", split_axis=1, concat_axis=0, tiled=True),
        lax.all_to_all(product, "ep", split_axis=1, concat_axis=0, tiled=True),
    )
    per_pair = back_rows.reshape(experts * capacity, width_part)[target]
    per_pair = per_pair.reshape(tok_count, top_count, width_part)
    token_grad = jnp.sum(per_pair.astype(jnp.float32), axis=1).astype(jnp.bfloat16)
    pair_product = back_product.reshape(experts * capacity)[target].reshape(tok_count, top_count)
    gate_grad = pair_product.astype(jnp.float32) / gates
    row_norms = jnp.stack(
        [
            jnp.sum(grad_gate * grad_gate, axis=-1),
            jnp.sum(grad_up * grad_up, axis=-1),
            jnp.sum(grad_down * grad_down, axis=-1),
        ],
        axis=0,
    )
    shared_term = jnp.einsum(
        "td,ts->ds", cotangent, shared_hidden, preferred_element_type=jnp.float32
    )
    grad_shared = lax.psum_scatter(shared_term, "ep", scatter_dimension=1, tiled=True)
    shared_norms = lax.psum(jnp.sum(grad_shared * grad_shared, axis=1), "ep")
    return (
        token_grad,
        gate_grad,
        grad_gate,
        grad_up,
        grad_down,
        row_norms,
        grad_shared,
        shared_norms,
    )


def solution(mesh):
    return jax.shard_map(
        on_device,
        mesh=mesh,
        in_specs=(
            P("ep", "tp"),
            P("ep", None),
            P("ep", None),
            P("ep", "tp"),
            P("ep", "tp", None),
            P("ep", "tp", None),
            P("ep", "tp", None),
            P("ep", None),
        ),
        out_specs=(
            P("ep", "tp"),
            P("ep", None),
            P("ep", "tp", None),
            P("ep", "tp", None),
            P("ep", "tp", None),
            P(None, "ep", "tp"),
            P("tp", "ep"),
            P("tp"),
        ),
        check_vma=False,
    )
```

profile of v0, /device:TPU:0, one launch (start us, length us, event | category | flops | bytes accessed | tf_op | source)
XLA Modules:
  0.0 189.0 jit_solution(876428887451017277)
XLA Ops:
  8.0 0.0 copy-start
  8.0 0.8 broadcast_multiply_fusion
  8.8 0.8 copy.30
  9.6 0.1 eq.29
  9.7 0.1 eq.25
  9.9 0.1 copy.29
  10.0 0.1 mul.79
  10.1 0.6 reduce-window.6
  10.7 0.2 slice_reduce_fusion
  11.0 0.1 fusion.55
  11.1 1.4 scatter_custom_fusion.1
  12.5 1.5 scatter_custom_fusion
  14.0 0.1 broadcast_in_dim.41
  14.1 0.0 copy-start.1
  14.1 1.2 mul.83
  15.3 0.5 mul.84
  15.9 0.1 copy.32
  16.0 0.1 mul.81
  16.1 2.1 %gather_fusion.1 = bf16[320,768]{1,0:T(8,128)(2,1)S(1)} fusion(bf16[128,768]{1,0:T(8,128)(2,1)S(1)} %copy-done.1, s32[1024]{0:T(1024)S(1)} %get-tuple-element.45), kind=kCustom, calls=%fused_computation.1 | custom fusion | bytes 984320 | tf_op jit(solution)/shard_map/gather | solution.py:42
  18.3 0.1 multiply_convert_fusion
  18.4 2.1 %gather_fusion = bf16[320,768]{1,0:T(8,128)(2,1)S(1)} fusion(bf16[256,768]{1,0:T(8,128)(2,1)S(1)} %multiply_convert_fusion, s32[1024]{0:T(1024)S(1)} %get-tuple-element.46), kind=kCustom, calls=%fused_computation | custom fusion | bytes 984320 | tf_op jit(solution)/shard_map/gather | solution.py:43
  20.5 0.9 broadcast_select_fusion
  21.4 20.8 %all_to_all.17 = bf16[8,40,768]{2,1,0:T(8,128)(2,1)S(1)} all-to-all(bf16[8,40,768]{2,1,0:T(8,128)(2,1)S(1)} %get-tuple-element.37), channel_id=1, replica_groups=mesh['ep'=8,'tp'=4] {'ep'}, dimensions={0} | all-to-all | bytes 983040 | tf_op jit(solution)/shard_map/all_to_all | solution.py:47
  42.2 3.5 %all-to-all-start = ((bf16[8,40,768]{2,1,0:T(8,128)(2,1)}), bf16[8,40,768]{2,1,0:T(8,128)(2,1)S(1)}, u32[]{:S(2)}, u32[]{:S(2)}) async-start(bf16[8,40,768]{2,1,0:T(8,128)(2,1)} %get-tuple-element.38), calls=%async_computation | async-start | bytes 983040 | tf_op jit(solution)/shard_map/all_to_all | solution.py:48
  45.7 0.0 all-reduce.3.cloned.1.call-start
  45.7 2.8 %fusion.28 = bf16[1,320,896]{2,1,0:T(8,128)(2,1)} fusion(bf16[320,768]{1,0:T(8,128)(2,1)S(1)} %bitcast.94, bf16[1,768,896]{2,1,0:T(8,128)(2,1)} %param.13), kind=kOutput, calls=%fused_computation.32 | convolution fusion | flops 440688640 | bytes 2441216 | tf_op jit(solution)/shard_map/erd,edf->erf/dot_general | solution.py:51
  48.6 1.5 fusion.25
  50.1 10.2 %all-to-all-done = bf16[8,40,768]{2,1,0:T(8,128)(2,1)S(1)} async-done(((bf16[8,40,768]{2,1,0:T(8,128)(2,1)}), bf16[8,40,768]{2,1,0:T(8,128)(2,1)S(1)}, u32[]{:S(2)}, u32[]{:S(2)}) %all-to-all-start) | async-done | bytes 491552 | tf_op jit(solution)/shard_map/all_to_all | solution.py:48
  60.2 3.0 %fusion.31 = bf16[1,320,896]{2,1,0:T(8,128)(2,1)} fusion(bf16[320,768]{1,0:T(8,128)(2,1)S(1)} %bitcast.98, bf16[1,768,896]{2,1,0:T(8,128)(2,1)} %param.14), kind=kOutput, calls=%fused_computation.33 | convolution fusion | flops 440688640 | bytes 2441216 | tf_op jit(solution)/shard_map/erd,edf->erf/dot_general | solution.py:52
  63.3 0.0 all-reduce.3.cloned.1.call-update
  63.3 0.0 reduce-scatter.2.cloned.1.call-start
  63.3 0.8 copy-done.2
  64.2 0.1 copy-done.13
  64.2 1.4 fusion.68
  65.7 0.0 reduce-scatter.2.cloned.1.call-update
  65.7 60.3 %all-reduce.3.cloned.1.call-done = (bf16[1,320,896]{2,1,0:T(8,128)(2,1)}, bf16[1,320,896]{2,1,0:T(8,128)(2,1)}, bf16[1,320,896]{2,1,0:T(8,128)(2,1)}) async-done(((bf16[1,320,896]{2,1,0:T(8,128)(2,1)}, bf16[1,320,896]{2,1,0:T(8,128)(2,1)}, bf16[1,320,896]{2,1,0:T(8,128)(2,1)}), (bf16[1,320,896]{2,1,0:T(8,128)(2,1)}, bf16[1,320,896]{2,1,0:T(8,128)(2,1)}, ...) | async-done | bytes 1720336 | tf_op jit(solution)/shard_map/psum | solution.py:56
  125.9 2.0 %fusion.41 = bf16[320]{0:T(512)(128)(2,1)S(1)} fusion(bf16[1,320,896]{2,1,0:T(8,128)(2,1)} %get-tuple-element.32, bf16[1,320,896]{2,1,0:T(8,128)(2,1)} %get-tuple-element.33, bf16[1,320,896]{2,1,0:T(8,128)(2,1)} %get-tuple-element.34), kind=kLoop, calls=%fused_computation.39 | loop fusion | flops 2866880 | bytes 1720960 | tf_op jit(solution)/shard_map/reduce_sum | solution.py:19
  128.0 0.7 convert_element_type.103
  128.7 4.6 %all-to-all-start.3 = ((bf16[1,8,40]{2,0,1:T(2,128)(2,1)}), bf16[1,8,40]{2,0,1:T(2,128)(2,1)S(1)}, u32[]{:S(2)}, u32[]{:S(2)}) async-start(bf16[1,8,40]{2,0,1:T(2,128)(2,1)} %convert_element_type.103), calls=%async_computation.3 | async-start | bytes 8192 | tf_op jit(solution)/shard_map/all_to_all | solution.py:70
  133.3 0.0 copy-start.15
  133.3 1.0 fusion
  134.4 0.3 copy-done.15
  134.7 0.9 fusion.34
  135.5 0.1 copy-done.12
  135.7 2.6 %multiply_reduce_fusion = (f32[768]{0:T(1024)S(1)}, f32[768,896]{1,0:T(8,128)}) fusion(bf16[320,768]{1,0:T(8,128)(2,1)S(1)} %bitcast.99, bf16[1,320,896]{2,1,0:T(8,128)(2,1)S(1)} %copy-done.5, bf16[1,320,896]{2,1,0:T(8,128)(2,1)S(1)} %copy-done.7), kind=kOutput, calls=%fused_computation.6 | convolution fusion | flops 444071168 | bytes 4393984 | tf_op jit(solution)/shard_map/erd,erf->edf/dot_general | solution.py:63
  138.3 0.8 copy.41
  139.1 0.5 broadcast.119
  139.6 3.7 %reduce.11 = bf16[320,768]{1,0:T(8,128)(2,1)S(1)} reduce(bf16[320,1,768]{2,1,0:T(2,128)(2,1)S(1)} %bitcast.90, bf16[]{:T(256)} %broadcast.119), dimensions={1}, to_apply=%bitcast.88.reduce_sub_computation | reduce | bytes 983042
  143.3 0.9 reshape.256
  144.2 5.1 %all-to-all-start.2 = ((bf16[8,2,15360]{2,1,0:T(2,128)(2,1)}), bf16[8,2,15360]{2,1,0:T(2,128)(2,1)S(1)}, u32[]{:S(2)}, u32[]{:S(2)}) async-start(bf16[8,2,15360]{2,1,0:T(2,128)(2,1)} %reshape.256), calls=%async_computation.2 | async-start | bytes 983040 | tf_op jit(solution)/shard_map/all_to_all | solution.py:69
  149.4 3.8 %multiply_reduce_fusion.1 = (f32[768]{0:T(1024)S(1)}, f32[768,896]{1,0:T(8,128)}) fusion(bf16[320,768]{1,0:T(8,128)(2,1)S(1)} %bitcast.96, bf16[1,320,896]{2,1,0:T(8,128)(2,1)S(1)} %copy-done.4, bf16[1,320,896]{2,1,0:T(8,128)(2,1)} %get-tuple-element.34), kind=kOutput, calls=%fused_computation.7 | convolution fusion | flops 444071168 | bytes 4393984 | tf_op jit(solution)/shard_map/erd,erf->edf/dot_general | solution.py:62
  153.2 2.7 %multiply_reduce_fusion.2 = (f32[768]{0:T(1024)S(1)}, f32[768,896]{1,0:T(8,128)}) fusion(bf16[320,768]{1,0:T(8,128)(2,1)S(1)} %bitcast.97, bf16[1,320,896]{2,1,0:T(8,128)(2,1)S(1)} %copy-done.8, bf16[1,320,896]{2,1,0:T(8,128)(2,1)S(1)} %copy-done.6, bf16[1,320,896]{2,1,0:T(8,128)(2,1)S(1)} %copy-done.4), kind=kOutput, calls=%fused_computation.8 | convolution fusion | flops 445504768 | bytes 4967424 | tf_op jit(solution)/shard_map/erd,erf->edf/dot_general | solution.py:59
  155.9 0.6 pad_maximum_fusion
  156.5 0.1 reshape.197
  156.6 1.9 %gather_fusion.3 = bf16[256]{0:T(256)(128)(2,1)S(1)} fusion(bf16[320]{0:T(512)(128)(2,1)S(1)} %reshape.197, s32[1024]{0:T(1024)S(1)} %pad_clamp_fusion), kind=kCustom, calls=%fused_computation.3 | custom fusion | bytes 2048 | tf_op jit(solution)/shard_map/gather | solution.py:75
  158.5 0.1 reshape.199
  158.7 0.6 copy.36
  159.4 0.9 multiply_reduce_fusion.3
  160.3 17.7 %psum.31 = f32[768]{0:T(1024)} all-reduce(f32[768]{0:T(1024)S(1)} %multiply_reduce_fusion.3), channel_id=1, replica_groups=mesh['ep'=8,'tp'=4] {'ep'}, use_global_device_ids=true, to_apply=%region_15.16 | all-reduce | flops 768 | bytes 6144 | tf_op jit(solution)/shard_map/psum | solution.py:89
  178.0 0.4 reshape.257
  178.4 0.1 copy.40
  178.5 1.2 gather_fusion.2
  179.7 0.2 reshape.196
  179.8 1.7 reduce_sum.70
  (42 shorter events, 0.2 us)
Async XLA Ops:
  8.0 40.6 %copy-start = (bf16[1,768,896]{2,1,0:T(8,128)(2,1)S(1)}, bf16[1,768,896]{2,1,0:T(8,128)(2,1)}, u32[]{:S(2)}) copy-start(bf16[1,768,896]{2,1,0:T(8,128)(2,1)} %param.12) | copy-start | bytes 4128772
  14.1 1.7 copy-start.14
  14.1 2.0 %copy-start.1 = (bf16[128,768]{1,0:T(8,128)(2,1)S(1)}, bf16[128,768]{1,0:T(8,128)(2,1)}, u32[]{:S(2)}) copy-start(bf16[128,768]{1,0:T(8,128)(2,1)} %param.8) | copy-start | bytes 589828
  42.2 6.4 %copy-start.9 = (bf16[8,40,768]{2,1,0:T(8,128)(2,1)}, bf16[8,40,768]{2,1,0:T(8,128)(2,1)S(1)}, u32[]{:S(2)}) copy-start(bf16[8,40,768]{2,1,0:T(8,128)(2,1)S(1)} %all_to_all.17) | copy-start | bytes 1474564
  42.2 18.0 %all-to-all-start = ((bf16[8,40,768]{2,1,0:T(8,128)(2,1)}), bf16[8,40,768]{2,1,0:T(8,128)(2,1)S(1)}, u32[]{:S(2)}, u32[]{:S(2)}) async-start(bf16[8,40,768]{2,1,0:T(8,128)(2,1)} %get-tuple-element.38), calls=%async_computation | async-start | bytes 983040 | tf_op jit(solution)/shard_map/all_to_all | solution.py:48
  45.7 80.2 %all-reduce.3.cloned.1.call-start = ((), (), s32[]{:S(2)}) async-start(), calls=%async_computation.6 | async-start | bytes 3440640 | tf_op jit(solution)/shard_map/psum | solution.py:56
  60.2 3.0 %copy-start.11 = (bf16[8,40,768]{2,1,0:T(8,128)(2,1)}, bf16[8,40,768]{2,1,0:T(8,128)(2,1)S(1)}, u32[]{:S(2)}) copy-start(bf16[8,40,768]{2,1,0:T(8,128)(2,1)S(1)} %all-to-all-done) | copy-start | bytes 1474564
  63.3 0.9 copy-start.2
  63.3 1.0 copy-start.13
  63.3 96.1 %reduce-scatter.2.cloned.1.call-start = ((), (), s32[]{:S(2)}) async-start(), calls=%async_computation.5 | async-start | bytes 1548288 | tf_op jit(solution)/shard_map/reduce_scatter | solution.py:88
  125.9 7.3 %copy-start.3 = (bf16[1,320,896]{2,1,0:T(8,128)(2,1)S(1)}, bf16[1,320,896]{2,1,0:T(8,128)(2,1)}, u32[]{:S(2)}) copy-start(bf16[1,320,896]{2,1,0:T(8,128)(2,1)} %get-tuple-element.32) | copy-start | bytes 1720324
  125.9 7.3 %copy-start.5 = (bf16[1,320,896]{2,1,0:T(8,128)(2,1)S(1)}, bf16[1,320,896]{2,1,0:T(8,128)(2,1)}, u32[]{:S(2)}) copy-start(bf16[1,320,896]{2,1,0:T(8,128)(2,1)} %get-tuple-element.33) | copy-start | bytes 1720324
  125.9 7.4 %copy-start.7 = (bf16[1,320,896]{2,1,0:T(8,128)(2,1)S(1)}, bf16[1,320,896]{2,1,0:T(8,128)(2,1)}, u32[]{:S(2)}) copy-start(bf16[1,320,896]{2,1,0:T(8,128)(2,1)} %get-tuple-element.34) | copy-start | bytes 1720324
  128.7 15.6 %all-to-all-start.3 = ((bf16[1,8,40]{2,0,1:T(2,128)(2,1)}), bf16[1,8,40]{2,0,1:T(2,128)(2,1)S(1)}, u32[]{:S(2)}, u32[]{:S(2)}) async-start(bf16[1,8,40]{2,0,1:T(2,128)(2,1)} %convert_element_type.103), calls=%async_computation.3 | async-start | bytes 8192 | tf_op jit(solution)/shard_map/all_to_all | solution.py:70
  133.3 1.3 copy-start.15
  134.7 1.0 copy-start.12
  143.3 6.0 %copy-start.4 = (bf16[1,320,896]{2,1,0:T(8,128)(2,1)S(1)}, bf16[1,320,896]{2,1,0:T(8,128)(2,1)}, u32[]{:S(2)}) copy-start(bf16[1,320,896]{2,1,0:T(8,128)(2,1)} %get-tuple-element.32) | copy-start | bytes 1720324
  143.3 6.0 %copy-start.10 = (bf16[8,40,768]{2,1,0:T(8,128)(2,1)S(1)}, bf16[8,40,768]{2,1,0:T(8,128)(2,1)}, u32[]{:S(2)}) copy-start(bf16[8,40,768]{2,1,0:T(8,128)(2,1)} %copy-done.9) | copy-start | bytes 1474564
  144.2 33.8 %all-to-all-start.2 = ((bf16[8,2,15360]{2,1,0:T(2,128)(2,1)}), bf16[8,2,15360]{2,1,0:T(2,128)(2,1)S(1)}, u32[]{:S(2)}, u32[]{:S(2)}) async-start(bf16[8,2,15360]{2,1,0:T(2,128)(2,1)} %reshape.256), calls=%async_computation.2 | async-start | bytes 983040 | tf_op jit(solution)/shard_map/all_to_all | solution.py:69
  149.4 3.8 %copy-start.6 = (bf16[1,320,896]{2,1,0:T(8,128)(2,1)S(1)}, bf16[1,320,896]{2,1,0:T(8,128)(2,1)}, u32[]{:S(2)}) copy-start(bf16[1,320,896]{2,1,0:T(8,128)(2,1)} %get-tuple-element.33) | copy-start | bytes 1720324
  149.4 3.8 %copy-start.8 = (bf16[1,320,896]{2,1,0:T(8,128)(2,1)S(1)}, bf16[1,320,896]{2,1,0:T(8,128)(2,1)}, u32[]{:S(2)}) copy-start(bf16[1,320,896]{2,1,0:T(8,128)(2,1)} %get-tuple-element.34) | copy-start | bytes 1720324
Sparse Core Ops, SparseCore 0:
  63.4 62.4 all-reduce.2
Sparse Core Ops, SparseCore 1:
  66.6 32.3 reduce-scatter.1
where the time goes:
time: 190 us; the launch traced here: 189 us
  waiting for transfers between devices  70.5 us (37%)
  blocking collectives  38.5 us (20%)
  matrix products  19.8 us (10%)
  local copies, waits for them, and re-layouts  19.6 us (10%)
  between operations  15.8 us (8%)
  starting transfers between devices  13.3 us (7%)
  other arithmetic  11.7 us (6%)
    psum x1, waiting for transfers between devices, on_device(): lax.psum(down_part.astype(jnp.bfloat16), 'tp').astype(jnp.float32)  60.3 us
    all_to_all x1, blocking collectives, on_device(): lax.all_to_all(token_rows, 'ep', split_axis=0, concat_axis=1, tiled=True)  20.8 us
    psum x1, blocking collectives, on_device(): shared_norms = lax.psum(jnp.sum(grad_shared * grad_shared, axis=1), 'ep')  17.7 us
    all_to_all x1, waiting for transfers between devices, on_device(): lax.all_to_all(grad_rows, 'ep', split_axis=0, concat_axis=1, tiled=True)  10.2 us
    all_to_all x1, starting transfers between devices, on_device(): lax.all_to_all(token_back, 'ep', split_axis=1, concat_axis=0, tiled=True)  5.09 us
    unnamed x39, local copies, waits for them, and re-layouts  4.82 us
    all_to_all x1, starting transfers between devices, on_device(): lax.all_to_all(product, 'ep', split_axis=1, concat_axis=0, tiled=True)  4.61 us
  transfers between devices with their start and end apart: 5, of which 2 were waited for; matrix products, arithmetic and copies ran while one was open for 16% of the time, Pallas kernels for 0%

commit v1 on v0

v1 whole, which is shorter than its diff:
```python
import functools

import jax
import jax.numpy as jnp
from jax import lax
from jax.experimental import pallas as pl
from jax.experimental.pallas import tpu as pltpu
from jax.sharding import PartitionSpec as P

MESH = pl.DeviceIdType.MESH
F32 = jnp.float32
BF16 = jnp.bfloat16


def round_up(n, m):
    return -(-n // m) * m


def dot(a, b, ca=1, cb=0):
    return lax.dot_general(a, b, (((ca,), (cb,)), ((), ())), preferred_element_type=F32)


def exchange_kernel(
    n_ep, n_tp, cap,
    tok, cot, rts, gts, gates, sh, wg_h, wu_h, wd_h,
    tg_out, gg_out, gs_out, sn_out, x_out, y_out, act_out,
    hot0, hot1, send_x, send_y, recv_x, recv_y, xs, ys, wg, wu, wd,
    sh_send, sh_recv, nr_send, nr_recv, part, rs_recv, act, prod, back_send, back_recv,
    w_sem, x_ss, x_rs, y_ss, y_rs, s_ss, s_rs, n_ss, n_rs, p_ss, p_rs, a_ss, a_rs,
    q_ss, q_rs, b_ss, b_rs, o_sem,
):
    me = lax.axis_index("ep")
    tp = lax.axis_index("tp")
    width = tok.shape[1]
    count = tok.shape[0]
    hid = wg.shape[1]
    rows = n_ep * cap
    chunk = rows // n_tp
    per_chunk = n_ep // n_tp
    wide = back_send.shape[2] - 128

    weight_copies = [
        pltpu.make_async_copy(h, v, w_sem.at[i])
        for i, (h, v) in enumerate(((wg_h, wg), (wu_h, wu), (wd_h, wd)))
    ]
    for c in weight_copies:
        c.start()

    barrier = pltpu.get_barrier_semaphore()
    for d in range(1, n_ep):
        pl.semaphore_signal(barrier, inc=1, device_id={"ep": lax.rem(me + d, n_ep)}, device_id_type=MESH)
    for d in range(1, n_tp):
        pl.semaphore_signal(barrier, inc=1, device_id={"tp": lax.rem(tp + d, n_tp)}, device_id_type=MESH)

    routes = rts[...]
    experts = lax.broadcasted_iota(jnp.int32, (n_ep, count), 0)
    pick = [(routes[k : k + 1, :] == experts).astype(F32) for k in range(2)]
    before = (
        lax.broadcasted_iota(jnp.int32, (count, count), 0)
        < lax.broadcasted_iota(jnp.int32, (count, count), 1)
    ).astype(BF16)
    earlier = dot((pick[0] + pick[1]).astype(BF16), before)
    row_ids = lax.broadcasted_iota(jnp.int32, (rows, count), 0)
    hits = []
    for k in range(2):
        slot = jnp.sum(pick[k] * earlier, axis=0, keepdims=True).astype(jnp.int32)
        hits.append(row_ids == routes[k : k + 1, :] * cap + slot)
    one = [jnp.where(h, 1.0, 0.0) for h in hits]
    hot0[...] = one[0].astype(BF16)
    hot1[...] = one[1].astype(BF16)
    both = (one[0] + one[1]).astype(BF16)
    gate_col = jnp.sum(
        jnp.where(hits[0], gts[0:1, :], 0.0) + jnp.where(hits[1], gts[1:2, :], 0.0),
        axis=1, keepdims=True,
    )
    send_x[...] = dot(both, tok[...]).reshape(n_ep, cap, width).astype(BF16)

    pl.semaphore_wait(barrier, n_ep - 1 + n_tp - 1)

    def to_ep(src, dst, ss, rs):
        copies = []
        for d in range(1, n_ep):
            peer = lax.rem(me + d, n_ep)
            c = pltpu.make_async_remote_copy(
                src_ref=src(peer), dst_ref=dst(me), send_sem=ss.at[d], recv_sem=rs.at[d],
                device_id={"ep": peer}, device_id_type=MESH,
            )
            c.start()
            copies.append(c)
        return copies

    def to_tp(src, dst, ss, rs):
        copies = []
        for d in range(1, n_tp):
            peer = lax.rem(tp + d, n_tp)
            c = pltpu.make_async_remote_copy(
                src_ref=src(peer), dst_ref=dst(d), send_sem=ss.at[d], recv_sem=rs.at[d],
                device_id={"tp": peer}, device_id_type=MESH,
            )
            c.start()
            copies.append(c)
        return copies

    x_copies = to_ep(lambda p: send_x.at[p], lambda m: recv_x.at[m], x_ss, x_rs)
    send_y[...] = (dot(both, cot[...]) * gate_col).reshape(n_ep, cap, width).astype(BF16)
    y_copies = to_ep(lambda p: send_y.at[p], lambda m: recv_y.at[m], y_ss, y_rs)
    recv_x[me] = send_x[me]
    recv_y[me] = send_y[me]

    depth = sh.shape[0] // n_ep
    sh_send[...] = dot(sh[...], cot[...]).reshape(n_ep, depth, width).astype(BF16)
    s_copies = to_ep(lambda p: sh_send.at[p], lambda m: sh_recv.at[m], s_ss, s_rs)
    sh_recv[me] = sh_send[me]

    for c in weight_copies:
        c.wait()
    for c in x_copies:
        c.wait_recv()
    xs[...] = recv_x[...].astype(F32).reshape(rows, width).astype(BF16)
    p_copies = []

    def partial(i, left, weight):
        part[i] = dot(left[...], weight[...]).astype(BF16).reshape(n_tp, chunk, hid)
        p_copies.append(
            to_tp(lambda p: part.at[i, p], lambda d: rs_recv.at[i, d], p_ss.at[i], p_rs.at[i])
        )

    partial(0, xs, wg)
    partial(1, xs, wu)
    for c in y_copies:
        c.wait_recv()
    ys[...] = recv_y[...].astype(F32).reshape(rows, width).astype(BF16)
    partial(2, ys, wd)
    out_copies = [
        pltpu.make_async_copy(xs, x_out, o_sem.at[0]),
        pltpu.make_async_copy(ys, y_out, o_sem.at[1]),
    ]
    for c in out_copies:
        c.start()

    sums = []
    for i in range(3):
        total = part[i, tp].astype(F32)
        for d in range(1, n_tp):
            p_copies[i][d - 1].wait_recv()
            total = total + rs_recv[i, d].astype(F32)
        sums.append(total)
    gate_sum, up_sum, down_sum = sums
    sigma = jax.nn.sigmoid(gate_sum)
    active = gate_sum * sigma
    act[1, tp] = (down_sum * up_sum * sigma * (1.0 + gate_sum * (1.0 - sigma))).astype(BF16)
    gb_copies = to_tp(lambda p: act.at[1, tp], lambda d: act.at[1, tp], a_ss.at[1], a_rs.at[1])
    act[2, tp] = (down_sum * active).astype(BF16)
    ub_copies = to_tp(lambda p: act.at[2, tp], lambda d: act.at[2, tp], a_ss.at[2], a_rs.at[2])
    hidden = active * up_sum
    product = jnp.sum(hidden * down_sum, axis=1, keepdims=True)
    prod[tp] = jnp.broadcast_to(product, (chunk, 128)).astype(BF16)
    q_copies = to_tp(lambda p: prod.at[tp], lambda d: prod.at[tp], q_ss, q_rs)
    act[0, tp] = hidden.astype(BF16)
    h_copies = to_tp(lambda p: act.at[0, tp], lambda d: act.at[0, tp], a_ss.at[0], a_rs.at[0])

    def back_copy(q, source):
        return pltpu.make_async_remote_copy(
            src_ref=back_send.at[q], dst_ref=back_recv.at[source], send_sem=b_ss.at[q],
            recv_sem=b_rs.at[source], device_id={"ep": q}, device_id_type=MESH,
        )

    def rows_back(j):
        out = dot(act[1, j], wg[...], 1, 1) + dot(act[2, j], wu[...], 1, 1)
        out = out.reshape(per_chunk, cap, width).astype(BF16)
        extra = prod[j].astype(F32).reshape(per_chunk, cap, 128).astype(BF16)
        for i in range(per_chunk):
            q = j * per_chunk + i
            if wide != width:
                back_send[q] = jnp.zeros((cap, wide + 128), BF16)
            back_send[q, :, :width] = out[i]
            back_send[q, :, wide:] = extra[i]

            @pl.when(q != me)
            def _():
                back_copy(q, me).start()

    rows_back(tp)

    for c in s_copies:
        c.wait_recv()
    shared = jnp.sum(sh_recv[...].astype(F32), axis=0)
    gs_out[...] = shared
    nr_send[...] = jnp.broadcast_to(jnp.sum(shared * shared, axis=0, keepdims=True), (8, width))
    n_copies = to_ep(lambda p: nr_send, lambda m: nr_recv.at[m], n_ss, n_rs)
    nr_recv[me] = nr_send[...]

    for d in range(1, n_tp):
        gb_copies[d - 1].wait_recv()
        ub_copies[d - 1].wait_recv()
        q_copies[d - 1].wait_recv()
        rows_back(lax.rem(tp + n_tp - d, n_tp))

    for d in range(1, n_tp):
        h_copies[d - 1].wait_recv()
    act_copy = pltpu.make_async_copy(act, act_out, o_sem.at[2])
    act_copy.start()
    for c in n_copies:
        c.wait_recv()
    sn_out[...] = jnp.sum(nr_recv[...], axis=0)
    back_recv[me] = back_send[me]
    for d in range(1, n_ep):
        source = lax.rem(me + n_ep - d, n_ep)
        back_copy(lax.rem(me + d, n_ep), source).wait_recv()
    back = back_recv[...].astype(F32).reshape(rows, wide + 128).astype(BF16)
    both = (hot0[...].astype(F32) + hot1[...].astype(F32)).astype(BF16)
    tg_out[...] = dot(both, back[:, :width], 0, 0).astype(BF16)
    first = dot(hot0[...], back[:, wide:], 0, 0)[:, :2]
    second = dot(hot1[...], back[:, wide:], 0, 0)[:, :2]
    lane = lax.broadcasted_iota(jnp.int32, (count, 2), 1)
    gg_out[...] = jnp.where(lane == 0, first, second) / gates[...]

    for group in (x_copies, y_copies, s_copies, n_copies, gb_copies, ub_copies, q_copies, h_copies, *p_copies):
        for c in group:
            c.wait_send()
    for d in range(1, n_ep):
        back_copy(lax.rem(me + d, n_ep), me).wait_send()
    for c in (*out_copies, act_copy):
        c.wait()


def grads_kernel(x, y, act, gg, gu, gd, norms):
    for i, (left, which, out) in enumerate(((x, 1, gg), (x, 2, gu), (y, 0, gd))):
        grad = dot(left[...], act[which], 0, 0)
        out[...] = grad
        norms[i, :] = jnp.sum(grad * grad, axis=1)


def on_device(n_ep, n_tp, tokens, routes, gates, cotangent, w_gate, w_up, w_down, shared_hidden):
    count, width = tokens.shape
    top = routes.shape[1]
    hid = w_gate.shape[2]
    cap = round_up(5 * count * top // (4 * n_ep), 8)
    rows = n_ep * cap
    chunk = rows // n_tp
    own = shared_hidden.shape[1] // n_ep
    depth = round_up(own, 16)
    wide = round_up(width, 128)
    sh = shared_hidden.T.reshape(n_ep, own, count)
    sh = jnp.pad(sh, ((0, 0), (0, depth - own), (0, 0))).reshape(n_ep * depth, count)
    vm = pl.BlockSpec(memory_space=pltpu.VMEM)
    hbm = pl.BlockSpec(memory_space=pl.ANY)
    dma = pltpu.SemaphoreType.DMA
    sds = jax.ShapeDtypeStruct
    tg, gg, gs, sn, x, y, act = pl.pallas_call(
        functools.partial(exchange_kernel, n_ep, n_tp, cap),
        out_shape=(
            sds((count, width), BF16), sds((count, top), F32), sds((depth, width), F32),
            sds((8, width), F32), sds((rows, width), BF16), sds((rows, width), BF16),
            sds((3, n_tp, chunk, hid), BF16),
        ),
        in_specs=[vm] * 6 + [hbm] * 3,
        out_specs=(vm, vm, vm, vm, hbm, hbm, hbm),
        scratch_shapes=[
            pltpu.VMEM((rows, count), BF16), pltpu.VMEM((rows, count), BF16),
            *[pltpu.VMEM((n_ep, cap, width), BF16)] * 4,
            *[pltpu.VMEM((rows, width), BF16)] * 2,
            *[pltpu.VMEM((width, hid), BF16)] * 3,
            *[pltpu.VMEM((n_ep, depth, width), BF16)] * 2,
            pltpu.VMEM((8, width), F32), pltpu.VMEM((n_ep, 8, width), F32),
            *[pltpu.VMEM((3, n_tp, chunk, hid), BF16)] * 3,
            pltpu.VMEM((n_tp, chunk, 128), BF16),
            *[pltpu.VMEM((n_ep, cap, wide + 128), BF16)] * 2,
            dma((3,)), *[dma((n_ep,))] * 8, *[dma((3, n_tp))] * 4, *[dma((n_tp,))] * 2,
            *[dma((n_ep,))] * 2, dma((3,)),
        ],
        compiler_params=pltpu.CompilerParams(
            collective_id=0, has_side_effects=True, vmem_limit_bytes=56 * 1024 * 1024
        ),
    )(tokens, cotangent, routes.T, gates.T, gates, sh, w_gate[0], w_up[0], w_down[0])
    act = act.reshape(3, rows, hid)
    tile = 256 if width % 256 == 0 else width
    grad_spec = pl.BlockSpec((tile, hid), lambda i: (i, 0))
    grad_gate, grad_up, grad_down, norms = pl.pallas_call(
        grads_kernel,
        grid=(width // tile,),
        out_shape=(*[sds((width, hid), F32)] * 3, sds((3, width), F32)),
        in_specs=[pl.BlockSpec((rows, tile), lambda i: (0, i))] * 2
        + [pl.BlockSpec((3, rows, hid), lambda i: (0, 0, 0))],
        out_specs=(grad_spec, grad_spec, grad_spec, pl.BlockSpec((3, tile), lambda i: (0, i))),
        compiler_params=pltpu.CompilerParams(vmem_limit_bytes=40 * 1024 * 1024),
    )(x, y, act)
    return (
        tg, gg, grad_gate[None], grad_up[None], grad_down[None], norms[:, None, :],
        gs[:own].T, sn[0],
    )


def solution(mesh):
    return jax.shard_map(
        functools.partial(on_device, mesh.shape["ep"], mesh.shape["tp"]),
        mesh=mesh,
        in_specs=(
            P("ep", "tp"),
            P("ep", None),
            P("ep", None),
            P("ep", "tp"),
            P("ep", "tp", None),
            P("ep", "tp", None),
            P("ep", "tp", None),
            P("ep", None),
        ),
        out_specs=(
            P("ep", "tp"),
            P("ep", None),
            P("ep", "tp", None),
            P("ep", "tp", None),
            P("ep", "tp", None),
            P(None, "ep", "tp"),
            P("tp", "ep"),
            P("tp"),
        ),
        check_vma=False,
    )
```

time: 190 us -> 92.3 us (0.49)
  the two profiles are of different devices: /device:TPU:0 before, /device:TPU:17 now
where the time goes in v1:
time: 92.3 us; the launch traced here: 91.9 us
  Pallas kernels  79 us (86%)
  local copies, waits for them, and re-layouts  12.2 us (13%)
    pallas_call x1, Pallas kernels, on_device(): pl.pallas_call(functools.partial(exchange_kernel, n_ep, n_tp, cap), out_s...  74.8 us
    unnamed x12, local copies, waits for them, and re-layouts  7.74 us
    pallas_call x1, Pallas kernels, on_device(): pl.pallas_call(grads_kernel, grid=(width // tile,), out_shape=(*[sds((wid...  4.21 us

profile of v1, /device:TPU:17, one launch (start us, length us, event | category | flops | bytes accessed | tf_op | source)
XLA Modules:
  0.0 91.9 jit_solution(6442024624931195162)
XLA Ops:
  0.6 1.4 %copy.16.gates = f32[128,2]{1,0:T(8,128)} copy(f32[128,2]{0,1:T(2,128)} %param.10) | data formatting | bytes 2048 | tf_op args[2]
  2.0 1.6 %pad.4 = bf16[8,64,128]{2,1,0:T(8,128)(2,1)} pad(bf16[8,56,128]{2,1,0:T(8,128)(2,1)} %bitcast.22, bf16[]{:T(256)} %constant.2.clone.1), padding=0_0x0_8x0_0 | pad | bytes 245762 | tf_op jit(solution)/shard_map/jit(_pad)/pad | solution.py:245
  3.6 74.8 %shard_map.143 = (bf16[128,768]{1,0:T(8,128)(2,1)}, f32[128,2]{1,0:T(8,128)}, f32[64,768]{1,0:T(8,128)}, f32[8,768]{1,0:T(8,128)}, bf16[320,768]{1,0:T(8,128)(2,...) custom-call(bf16[128,768]{1,0:T(8,128)(2,1)} %tok.1, bf16[128,768]{1,0:T(8,128)(2,1)} %cot.1, ...), custom_call_target="tpu_custom_call" | custom-call | tf_op jit(solution)/shard_map/pallas_call | solution.py:250
  78.4 0.0 copy-start.3
  78.4 1.5 %copy.17 = f32[128,2]{0,1:T(2,128)} copy(f32[128,2]{1,0:T(8,128)} %get-tuple-element.31) | data formatting | bytes 2048
  79.9 1.3 %slice_reduce_fusion = f32[768]{0:T(1024)} fusion(f32[8,768]{1,0:T(8,128)} %get-tuple-element.29), kind=kLoop, calls=%fused_computation.1 | loop fusion | bytes 6144 | tf_op jit(solution)/shard_map/slice | solution.py:290
  81.3 1.6 %slice_bitcast_fusion = f32[768,56]{0,1:T(8,128)} fusion(f32[64,768]{1,0:T(8,128)} %get-tuple-element.28), kind=kLoop, calls=%fused_computation | loop fusion | bytes 344064 | tf_op jit(solution)/shard_map/transpose | solution.py:290
  82.8 0.0 copy-start
  82.9 1.5 %copy-done = bf16[3,4,80,896]{3,2,1,0:T(8,128)(2,1)S(1)} copy-done((bf16[3,4,80,896]{3,2,1,0:T(8,128)(2,1)S(1)}, bf16[3,4,80,896]{3,2,1,0:T(8,128)(2,1)}, u32[]{:S(2)}) %copy-start) | copy-done | bytes 1720344
  84.3 0.0 copy-start.1
  84.3 1.0 %copy-done.1 = bf16[320,768]{1,0:T(8,128)(2,1)S(1)} copy-done((bf16[320,768]{1,0:T(8,128)(2,1)S(1)}, bf16[320,768]{1,0:T(8,128)(2,1)}, u32[]{:S(2)}) %copy-start.1) | copy-done | bytes 491544
  85.3 0.0 copy-start.2
  85.3 1.0 %copy-done.2 = bf16[320,768]{1,0:T(8,128)(2,1)S(1)} copy-done((bf16[320,768]{1,0:T(8,128)(2,1)S(1)}, bf16[320,768]{1,0:T(8,128)(2,1)}, u32[]{:S(2)}) %copy-start.2) | copy-done | bytes 491544
  86.4 4.2 %shard_map.144 = (f32[768,896]{1,0:T(8,128)}, f32[768,896]{1,0:T(8,128)}, f32[768,896]{1,0:T(8,128)}, f32[3,768]{1,0:T(4,128)S(1)}) custom-call(bf16[320,768]{1,0:T(8,128)(2,1)S(1)} %copy-done.1, bf16[320,768]{1,0:T(8,128)(2,1)S(1)} %copy-done.2, bf16[3,320,896]{2,1,0:T(8,128)(2,1)S(1)} %bitcast.16), custom_call_target="tpu_custom_call" | custom-call | tf_op jit(solution)/shard_map/pallas_call | solution.py:279
  90.6 0.6 copy.18
  91.2 0.0 copy-done.3
  91.2 0.7 copy.20
Async XLA Ops:
  78.4 12.8 %copy-start.3 = (bf16[128,768]{1,0:T(8,128)(2,1)S(1)}, bf16[128,768]{1,0:T(8,128)(2,1)}, u32[]{:S(2)}) copy-start(bf16[128,768]{1,0:T(8,128)(2,1)} %get-tuple-element.46) | copy-start | bytes 589828
  82.8 1.5 %copy-start = (bf16[3,4,80,896]{3,2,1,0:T(8,128)(2,1)S(1)}, bf16[3,4,80,896]{3,2,1,0:T(8,128)(2,1)}, u32[]{:S(2)}) copy-start(bf16[3,4,80,896]{3,2,1,0:T(8,128)(2,1)} %get-tuple-element.23) | copy-start | bytes 5160964
  84.3 1.0 %copy-start.1 = (bf16[320,768]{1,0:T(8,128)(2,1)S(1)}, bf16[320,768]{1,0:T(8,128)(2,1)}, u32[]{:S(2)}) copy-start(bf16[320,768]{1,0:T(8,128)(2,1)} %get-tuple-element.21.x) | copy-start | bytes 1474564
  85.3 1.0 %copy-start.2 = (bf16[320,768]{1,0:T(8,128)(2,1)S(1)}, bf16[320,768]{1,0:T(8,128)(2,1)}, u32[]{:S(2)}) copy-start(bf16[320,768]{1,0:T(8,128)(2,1)} %get-tuple-element.22.y) | copy-start | bytes 1474564

commit v2 on v1

--- a/solution.py
+++ b/solution.py
@@ -22,7 +22,7 @@
 
 def exchange_kernel(
     n_ep, n_tp, cap,
-    tok, cot, rts, gts, gates, sh, wg_h, wu_h, wd_h,
+    tok, cot, rts, gts, sh, wg_h, wu_h, wd_h,
     tg_out, gg_out, gs_out, sn_out, x_out, y_out, act_out,
     hot0, hot1, send_x, send_y, recv_x, recv_y, xs, ys, wg, wu, wd,
     sh_send, sh_recv, nr_send, nr_recv, part, rs_recv, act, prod, back_send, back_recv,
@@ -125,12 +125,46 @@
             to_tp(lambda p: part.at[i, p], lambda d: rs_recv.at[i, d], p_ss.at[i], p_rs.at[i])
         )
 
-    partial(0, xs, wg)
-    partial(1, xs, wu)
+    def pair_copy(src, dst, peer, ss, rs):
+        c = pltpu.make_async_remote_copy(
+            src_ref=src, dst_ref=dst, send_sem=ss, recv_sem=rs,
+            device_id={"tp": peer}, device_id_type=MESH,
+        )
+        c.start()
+        return c
+
+    square = n_tp == 4
+    x_peer = tp + 1 - 2 * lax.rem(tp, 2)
+    y_peer = lax.rem(tp + 2, n_tp)
+    across = lax.rem(x_peer + 2, n_tp)
+    turns = ((x_peer, y_peer), (y_peer, x_peer))
+
+    def paired(i, left, weight):
+        part[i] = dot(left[...], weight[...]).astype(BF16).reshape(n_tp, chunk, hid)
+        near = turns[i][0]
+        p_copies.append([
+            pair_copy(part.at[i, across], rs_recv.at[i, 1], near, p_ss.at[i, 1], p_rs.at[i, 1]),
+            pair_copy(part.at[i, near], rs_recv.at[i, 0], near, p_ss.at[i, 0], p_rs.at[i, 0]),
+        ])
+
+    def paired_pass(i):
+        far = turns[i][1]
+        p_copies[i][0].wait_recv()
+        rs_recv[i, 3] = (part[i, far].astype(F32) + rs_recv[i, 1].astype(F32)).astype(BF16)
+        p_copies[i].append(
+            pair_copy(rs_recv.at[i, 3], rs_recv.at[i, 2], far, p_ss.at[i, 2], p_rs.at[i, 2])
+        )
+
+    first_step = paired if square else partial
+    first_step(0, xs, wg)
+    first_step(1, xs, wu)
     for c in y_copies:
         c.wait_recv()
     ys[...] = recv_y[...].astype(F32).reshape(rows, width).astype(BF16)
     partial(2, ys, wd)
+    if square:
+        paired_pass(0)
+        paired_pass(1)
     out_copies = [
         pltpu.make_async_copy(xs, x_out, o_sem.at[0]),
         pltpu.make_async_copy(ys, y_out, o_sem.at[1]),
@@ -141,6 +175,11 @@
     sums = []
     for i in range(3):
         total = part[i, tp].astype(F32)
+        if square and i < 2:
+            for c in p_copies[i][1:]:
+                c.wait_recv()
+            sums.append(total + rs_recv[i, 0].astype(F32) + rs_recv[i, 2].astype(F32))
+            continue
         for d in range(1, n_tp):
             p_copies[i][d - 1].wait_recv()
             total = total + rs_recv[i, d].astype(F32)
@@ -149,9 +188,24 @@
     sigma = jax.nn.sigmoid(gate_sum)
     active = gate_sum * sigma
     act[1, tp] = (down_sum * up_sum * sigma * (1.0 + gate_sum * (1.0 - sigma))).astype(BF16)
-    gb_copies = to_tp(lambda p: act.at[1, tp], lambda d: act.at[1, tp], a_ss.at[1], a_rs.at[1])
+    def spread(i):
+        if not square:
+            return to_tp(lambda p: act.at[i, tp], lambda d: act.at[i, tp], a_ss.at[i], a_rs.at[i])
+        return [
+            pair_copy(act.at[i, tp], act.at[i, tp], peer, a_ss.at[i, k], a_rs.at[i, k])
+            for k, peer in enumerate(turns[i - 1])
+        ]
+
+    def relay(i, copies):
+        near, far = turns[i - 1]
+        copies[0].wait_recv()
+        copies.append(
+            pair_copy(act.at[i, near], act.at[i, near], far, a_ss.at[i, 2], a_rs.at[i, 2])
+        )
+
+    gb_copies = spread(1)
     act[2, tp] = (down_sum * active).astype(BF16)
-    ub_copies = to_tp(lambda p: act.at[2, tp], lambda d: act.at[2, tp], a_ss.at[2], a_rs.at[2])
+    ub_copies = spread(2)
     hidden = active * up_sum
     product = jnp.sum(hidden * down_sum, axis=1, keepdims=True)
     prod[tp] = jnp.broadcast_to(product, (chunk, 128)).astype(BF16)
@@ -181,20 +235,34 @@
                 back_copy(q, me).start()
 
     rows_back(tp)
+    if square:
+        relay(1, gb_copies)
+        relay(2, ub_copies)
 
     for c in s_copies:
         c.wait_recv()
     shared = jnp.sum(sh_recv[...].astype(F32), axis=0)
-    gs_out[...] = shared
+    gs_out[...] = shared[: gs_out.shape[0]]
     nr_send[...] = jnp.broadcast_to(jnp.sum(shared * shared, axis=0, keepdims=True), (8, width))
     n_copies = to_ep(lambda p: nr_send, lambda m: nr_recv.at[m], n_ss, n_rs)
     nr_recv[me] = nr_send[...]
 
-    for d in range(1, n_tp):
-        gb_copies[d - 1].wait_recv()
-        ub_copies[d - 1].wait_recv()
-        q_copies[d - 1].wait_recv()
-        rows_back(lax.rem(tp + n_tp - d, n_tp))
+    if square:
+        for c in q_copies:
+            c.wait_recv()
+        ub_copies[1].wait_recv()
+        rows_back(x_peer)
+        gb_copies[1].wait_recv()
+        rows_back(y_peer)
+        gb_copies[2].wait_recv()
+        ub_copies[2].wait_recv()
+        rows_back(across)
+    else:
+        for d in range(1, n_tp):
+            gb_copies[d - 1].wait_recv()
+            ub_copies[d - 1].wait_recv()
+            q_copies[d - 1].wait_recv()
+            rows_back(lax.rem(tp + n_tp - d, n_tp))
 
     for d in range(1, n_tp):
         h_copies[d - 1].wait_recv()
@@ -210,10 +278,8 @@
     back = back_recv[...].astype(F32).reshape(rows, wide + 128).astype(BF16)
     both = (hot0[...].astype(F32) + hot1[...].astype(F32)).astype(BF16)
     tg_out[...] = dot(both, back[:, :width], 0, 0).astype(BF16)
-    first = dot(hot0[...], back[:, wide:], 0, 0)[:, :2]
-    second = dot(hot1[...], back[:, wide:], 0, 0)[:, :2]
-    lane = lax.broadcasted_iota(jnp.int32, (count, 2), 1)
-    gg_out[...] = jnp.where(lane == 0, first, second) / gates[...]
+    for k, hot in enumerate((hot0, hot1)):
+        gg_out[k : k + 1, :] = dot(back[:, wide:], hot[...], 0, 0)[0:1, :] / gts[k : k + 1, :]
 
     for group in (x_copies, y_copies, s_copies, n_copies, gb_copies, ub_copies, q_copies, h_copies, *p_copies):
         for c in group:
@@ -224,11 +290,18 @@
         c.wait()
 
 
-def grads_kernel(x, y, act, gg, gu, gd, norms):
+def grads_kernel(x, y, act, tg, pg, gs, sn, gg, gu, gd, norms, tg_out, pg_out, gs_out, sn_out):
+    @pl.when(pl.program_id(0) == 0)
+    def _():
+        tg_out[...] = tg[...]
+        pg_out[...] = pg[...]
+        gs_out[...] = gs[...]
+        sn_out[...] = sn[0, :]
+
     for i, (left, which, out) in enumerate(((x, 1, gg), (x, 2, gu), (y, 0, gd))):
         grad = dot(left[...], act[which], 0, 0)
         out[...] = grad
-        norms[i, :] = jnp.sum(grad * grad, axis=1)
+        norms[i, 0, :] = jnp.sum(grad * grad, axis=1)
 
 
 def on_device(n_ep, n_tp, tokens, routes, gates, cotangent, w_gate, w_up, w_down, shared_hidden):
@@ -239,10 +312,12 @@
     rows = n_ep * cap
     chunk = rows // n_tp
     own = shared_hidden.shape[1] // n_ep
-    depth = round_up(own, 16)
+    depth = round_up(own, 8)
     wide = round_up(width, 128)
     sh = shared_hidden.T.reshape(n_ep, own, count)
-    sh = jnp.pad(sh, ((0, 0), (0, depth - own), (0, 0))).reshape(n_ep * depth, count)
+    if depth != own:
+        sh = jnp.pad(sh, ((0, 0), (0, depth - own), (0, 0)))
+    sh = sh.reshape(n_ep * depth, count)
     vm = pl.BlockSpec(memory_space=pltpu.VMEM)
     hbm = pl.BlockSpec(memory_space=pl.ANY)
     dma = pltpu.SemaphoreType.DMA
@@ -250,11 +325,11 @@
     tg, gg, gs, sn, x, y, act = pl.pallas_call(
         functools.partial(exchange_kernel, n_ep, n_tp, cap),
         out_shape=(
-            sds((count, width), BF16), sds((count, top), F32), sds((depth, width), F32),
+            sds((count, width), BF16), sds((top, count), F32), sds((own, width), F32),
             sds((8, width), F32), sds((rows, width), BF16), sds((rows, width), BF16),
             sds((3, n_tp, chunk, hid), BF16),
         ),
-        in_specs=[vm] * 6 + [hbm] * 3,
+        in_specs=[vm] * 5 + [hbm] * 3,
         out_specs=(vm, vm, vm, vm, hbm, hbm, hbm),
         scratch_shapes=[
             pltpu.VMEM((rows, count), BF16), pltpu.VMEM((rows, count), BF16),
@@ -266,28 +341,35 @@
             *[pltpu.VMEM((3, n_tp, chunk, hid), BF16)] * 3,
             pltpu.VMEM((n_tp, chunk, 128), BF16),
             *[pltpu.VMEM((n_ep, cap, wide + 128), BF16)] * 2,
-            dma((3,)), *[dma((n_ep,))] * 8, *[dma((3, n_tp))] * 4, *[dma((n_tp,))] * 2,
+            dma((3,)), *[dma((n_ep,))] * 8, *[dma((3, max(n_tp, 4)))] * 4, *[dma((n_tp,))] * 2,
             *[dma((n_ep,))] * 2, dma((3,)),
         ],
         compiler_params=pltpu.CompilerParams(
             collective_id=0, has_side_effects=True, vmem_limit_bytes=56 * 1024 * 1024
         ),
-    )(tokens, cotangent, routes.T, gates.T, gates, sh, w_gate[0], w_up[0], w_down[0])
+    )(tokens, cotangent, routes.T, gates.T, sh, w_gate[0], w_up[0], w_down[0])
     act = act.reshape(3, rows, hid)
     tile = 256 if width % 256 == 0 else width
     grad_spec = pl.BlockSpec((tile, hid), lambda i: (i, 0))
-    grad_gate, grad_up, grad_down, norms = pl.pallas_call(
+    whole = [pl.BlockSpec(a.shape, lambda i: (0, 0)) for a in (tg, gg, gs, sn)]
+    grad_gate, grad_up, grad_down, norms, tg, gg, gs, sn = pl.pallas_call(
         grads_kernel,
         grid=(width // tile,),
-        out_shape=(*[sds((width, hid), F32)] * 3, sds((3, width), F32)),
+        out_shape=(
+            *[sds((width, hid), F32)] * 3, sds((3, 1, width), F32), sds(tg.shape, BF16),
+            sds(gg.shape, F32), sds(gs.shape, F32), sds((width,), F32),
+        ),
         in_specs=[pl.BlockSpec((rows, tile), lambda i: (0, i))] * 2
-        + [pl.BlockSpec((3, rows, hid), lambda i: (0, 0, 0))],
-        out_specs=(grad_spec, grad_spec, grad_spec, pl.BlockSpec((3, tile), lambda i: (0, i))),
-        compiler_params=pltpu.CompilerParams(vmem_limit_bytes=40 * 1024 * 1024),
-    )(x, y, act)
+        + [pl.BlockSpec((3, rows, hid), lambda i: (0, 0, 0))] + whole,
+        out_specs=(
+            grad_spec, grad_spec, grad_spec, pl.BlockSpec((3, 1, tile), lambda i: (0, 0, i)),
+            *whole[:3], pl.BlockSpec((width,), lambda i: (0,)),
+        ),
+        compiler_params=pltpu.CompilerParams(vmem_limit_bytes=63 * 1024 * 1024),
+    )(x, y, act, tg, gg, gs, sn)
     return (
-        tg, gg, grad_gate[None], grad_up[None], grad_down[None], norms[:, None, :],
-        gs[:own].T, sn[0],
+        tg, gg.T, grad_gate[None], grad_up[None], grad_down[None], norms,
+        gs.T, sn,
     )
 
 

time: 92.3 us -> 81.5 us (0.88)
  the two profiles are of different devices: /device:TPU:17 before, /device:TPU:25 now
where the time goes in v2:
time: 81.5 us; the launch traced here: 81.3 us
  Pallas kernels  80.7 us (99%)
    pallas_call x1, Pallas kernels, on_device(): pl.pallas_call(functools.partial(exchange_kernel, n_ep, n_tp, cap), out_s...  74 us
    pallas_call x1, Pallas kernels, on_device(): pl.pallas_call(grads_kernel, grid=(width // tile,), out_shape=(*[sds((wid...  6.65 us

profile of v2, /device:TPU:25, one launch (start us, length us, event | category | flops | bytes accessed | tf_op | source)
XLA Modules:
  0.0 81.3 jit_solution(16322780113982993307)
XLA Ops:
  0.6 74.0 %shard_map.143 = (bf16[128,768]{1,0:T(8,128)(2,1)}, f32[2,128]{1,0:T(2,128)}, f32[56,768]{1,0:T(8,128)}, f32[8,768]{1,0:T(8,128)}, bf16[320,768]{1,0:T(8,128)(2,...) custom-call(bf16[128,768]{1,0:T(8,128)(2,1)} %tok.1, bf16[128,768]{1,0:T(8,128)(2,1)} %cot.1, ...), custom_call_target="tpu_custom_call" | custom-call | tf_op jit(solution)/shard_map/pallas_call | solution.py:325
  74.7 6.6 %shard_map.144 = (f32[768,896]{1,0:T(8,128)}, f32[768,896]{1,0:T(8,128)}, f32[768,896]{1,0:T(8,128)}, f32[3,1,768]{2,1,0:T(1,128)}, bf16[128,768]{1,0:T(8,128)(2...) custom-call(bf16[320,768]{1,0:T(8,128)(2,1)} %get-tuple-element.23.x, ...), custom_call_target="tpu_custom_call" | custom-call | tf_op jit(solution)/shard_map/pallas_call | solution.py:355

commit v3 on v2

--- a/solution.py
+++ b/solution.py
@@ -158,13 +158,13 @@
     first_step = paired if square else partial
     first_step(0, xs, wg)
     first_step(1, xs, wu)
+    if square:
+        paired_pass(0)
+        paired_pass(1)
     for c in y_copies:
         c.wait_recv()
     ys[...] = recv_y[...].astype(F32).reshape(rows, width).astype(BF16)
     partial(2, ys, wd)
-    if square:
-        paired_pass(0)
-        paired_pass(1)
     out_copies = [
         pltpu.make_async_copy(xs, x_out, o_sem.at[0]),
         pltpu.make_async_copy(ys, y_out, o_sem.at[1]),
@@ -211,7 +211,6 @@
     prod[tp] = jnp.broadcast_to(product, (chunk, 128)).astype(BF16)
     q_copies = to_tp(lambda p: prod.at[tp], lambda d: prod.at[tp], q_ss, q_rs)
     act[0, tp] = hidden.astype(BF16)
-    h_copies = to_tp(lambda p: act.at[0, tp], lambda d: act.at[0, tp], a_ss.at[0], a_rs.at[0])
 
     def back_copy(q, source):
         return pltpu.make_async_remote_copy(
@@ -238,6 +237,7 @@
     if square:
         relay(1, gb_copies)
         relay(2, ub_copies)
+    h_copies = to_tp(lambda p: act.at[0, tp], lambda d: act.at[0, tp], a_ss.at[0], a_rs.at[0])
 
     for c in s_copies:
         c.wait_recv()

time: 81.5 us -> 78 us (0.957)
  Pallas kernels: 80.7 us -> 77.1 us
    pallas_call x1, Pallas kernels: 74 us -> 70.5 us  [on_device(): pl.pallas_call(functools.partial(exchange_kernel, n_ep, n_tp, cap), out_s...]
where the time goes in v3:
time: 78 us; the launch traced here: 77.8 us
  Pallas kernels  77.1 us (99%)
    pallas_call x1, Pallas kernels, on_device(): pl.pallas_call(functools.partial(exchange_kernel, n_ep, n_tp, cap), out_s...  70.5 us
    pallas_call x1, Pallas kernels, on_device(): pl.pallas_call(grads_kernel, grid=(width // tile,), out_shape=(*[sds((wid...  6.65 us

profile of v3, /device:TPU:25, one launch (start us, length us, event | category | flops | bytes accessed | tf_op | source)
XLA Modules:
  0.0 77.8 jit_solution(1676049801581409978)
XLA Ops:
  0.6 70.5 %shard_map.143 = (bf16[128,768]{1,0:T(8,128)(2,1)}, f32[2,128]{1,0:T(2,128)}, f32[56,768]{1,0:T(8,128)}, f32[8,768]{1,0:T(8,128)}, bf16[320,768]{1,0:T(8,128)(2,...) custom-call(bf16[128,768]{1,0:T(8,128)(2,1)} %tok.1, bf16[128,768]{1,0:T(8,128)(2,1)} %cot.1, ...), custom_call_target="tpu_custom_call" | custom-call | tf_op jit(solution)/shard_map/pallas_call | solution.py:325
  71.1 6.6 %shard_map.144 = (f32[768,896]{1,0:T(8,128)}, f32[768,896]{1,0:T(8,128)}, f32[768,896]{1,0:T(8,128)}, f32[3,1,768]{2,1,0:T(1,128)}, bf16[128,768]{1,0:T(8,128)(2...) custom-call(bf16[320,768]{1,0:T(8,128)(2,1)} %get-tuple-element.23.x, ...), custom_call_target="tpu_custom_call" | custom-call | tf_op jit(solution)/shard_map/pallas_call | solution.py:355
